TPU v7x, 32 devices: a whole 2x2x4 slice. The times are simulated.
32 devices in a mesh: fs: 8 (over z, x), tp: 4 (over y, core).
Axes of the slice: x: 2, y: 2, z: 4, core: 2. Of those that a mesh axis runs over, the one named last changes fastest.
Arguments:
- stream: bfloat16 [4096, 2048], P('fs', 'tp'), may hold values from -6 to 6
- gain_mix: float32 [2048], replicated, may hold values from 0.1 to 1.9
- pool_weight: bfloat16 [4, 512, 512], P(None, 'fs', 'tp'), may hold values from -0.25 to 0.25
- pool_gain: float32 [2048], replicated, may hold values from 0.1 to 1.9
- gain_ffn: float32 [2048], replicated, may hold values from 0.1 to 1.9
- gate_weight: bfloat16 [2048, 5632], P('fs', 'tp'), may hold values from -0.125 to 0.125
- up_weight: bfloat16 [2048, 5632], P('fs', 'tp'), may hold values from -0.125 to 0.125
- gate_taps: float32 [3, 5632], replicated, may hold values from -2.5 to 2.5
- up_taps: float32 [3, 5632], replicated, may hold values from -2.5 to 2.5
- down_weight: bfloat16 [5632, 2048], P('tp', 'fs'), may hold values from -0.078125 to 0.078125
Outputs:
- layer_out: bfloat16 [4096, 2048], P('fs', 'tp')
All inputs are finite; a program needn't handle non-finite values.
Results may differ from a plain program's by a relative error of at most 0.01.
Values may be sent and summed in bfloat16 or wider, within the bound.
A program may use at most 64 MiB of HBM per device.

v0:
```python
import jax
import jax.numpy as jnp
from jax import lax
from jax.sharding import PartitionSpec as P

LEN = 128


epsilon = 1e-06


def rms_norm(values, scales):
    return values * lax.rsqrt(jnp.mean(values * values, axis=-1, keepdims=True) + epsilon) * scales


def delayed(values, amount):
    return jnp.pad(values, ((0, 0), (amount, 0), (0, 0)))[:, : values.shape[1]]


def pool_less(values):
    channels = values.shape[2]
    group_id = jnp.arange(channels) % 4
    partials = [values]
    running = values
    for amount in (1, 2, 4, 8):
        running = running + delayed(running, amount)
        partials.append(running)
    picked = jnp.where(
        group_id == 0,
        partials[1],
        jnp.where(group_id == 1, partials[2], jnp.where(group_id == 2, partials[3], partials[4])),
    )
    extent = jnp.where(
        group_id == 0, 2.0, jnp.where(group_id == 1, 4.0, jnp.where(group_id == 2, 8.0, 16.0))
    )
    position = jnp.arange(values.shape[1]).astype(jnp.float32)[:, None] + 1.0
    divisor = jnp.minimum(position, extent[None, :])
    return picked / divisor[None] - values


def causal_taps(values, kernel):
    reach = kernel.shape[0]
    length = values.shape[1]
    padded = jnp.pad(values, ((0, 0), (reach - 1, 0), (0, 0)))
    running = padded[:, 0:length] * kernel[0]
    for shift_by in range(1, reach):
        running = running + padded[:, shift_by : shift_by + length] * kernel[shift_by]
    return running


def add_rows(left, portion):
    return jnp.dot(left, portion, preferred_element_type=jnp.float32)


def body(
    stream,
    gain_mix,
    pool_weight,
    pool_gain,
    gain_ffn,
    gate_weight,
    up_weight,
    gate_taps,
    up_taps,
    down_weight,
):
    tok_rows, own_cols = stream.shape
    seq_count = tok_rows // LEN
    gathered = lax.all_gather(stream, "tp", axis=1, tiled=True)
    channels = gathered.shape[1]
    normed = lax.optimization_barrier(
        rms_norm(gathered.astype(jnp.float32), gain_mix).astype(jnp.bfloat16)
    )
    pooled = pool_less(normed.astype(jnp.float32).reshape(seq_count, LEN, channels)).astype(
        jnp.bfloat16
    )
    pooled = pooled.reshape(tok_rows, channels // 4, 4)
    pool_part = lax.all_gather(pool_weight, "fs", axis=1, tiled=True)
    pool_full = lax.all_gather(pool_part, "tp", axis=2, tiled=True)
    mixer = (
        jnp.einsum("tcg,gce->teg", pooled, pool_full, preferred_element_type=jnp.float32).reshape(
            tok_rows, channels
        )
        * pool_gain
    )
    middle = lax.optimization_barrier((gathered.astype(jnp.float32) + mixer).astype(jnp.bfloat16))
    normed_ffn = rms_norm(middle.astype(jnp.float32), gain_ffn).astype(jnp.bfloat16)
    hidden_cols = gate_weight.shape[1]

    def add_single(portion):
        return add_rows(normed_ffn, portion)

    gate_sum = add_single(lax.all_gather(gate_weight, "fs", axis=0, tiled=True))
    value_sum = add_single(lax.all_gather(up_weight, "fs", axis=0, tiled=True))
    gate_proj = lax.optimization_barrier(gate_sum.astype(jnp.bfloat16))
    value_proj = lax.optimization_barrier(value_sum.astype(jnp.bfloat16))
    column_start = lax.axis_index("tp") * hidden_cols
    gate_kernel = lax.dynamic_slice_in_dim(gate_taps, column_start, hidden_cols, 1)
    value_kernel = lax.dynamic_slice_in_dim(up_taps, column_start, hidden_cols, 1)
    gate_conv = causal_taps(
        gate_proj.astype(jnp.float32).reshape(seq_count, LEN, hidden_cols), gate_kernel
    )
    value_conv = causal_taps(
        value_proj.astype(jnp.float32).reshape(seq_count, LEN, hidden_cols), value_kernel
    )
    hidden = (
        (jax.nn.silu(gate_conv) * value_conv).astype(jnp.bfloat16).reshape(tok_rows, hidden_cols)
    )
    partial_value = jnp.dot(
        hidden,
        lax.all_gather(down_weight, "fs", axis=1, tiled=True),
        preferred_element_type=jnp.float32,
    )
    return lax.psum_scatter(partial_value, "tp", scatter_dimension=1, tiled=True).astype(
        jnp.bfloat16
    )


def solution(mesh):
    return jax.shard_map(
        body,
        mesh=mesh,
        in_specs=(
            P("fs", "tp"),
            P(),
            P(None, "fs", "tp"),
            P(),
            P(),
            P("fs", "tp"),
            P("fs", "tp"),
            P(),
            P(),
            P("tp", "fs"),
        ),
        out_specs=P("fs", "tp"),
        check_vma=False,
    )
```

profile of v0, /device:TPU:21, one launch (start us, length us, event | category | flops | bytes accessed | tf_op | source)
XLA Modules:
  0.0 405.3 jit_solution(10271177089141165696)
XLA Ops:
  6.5 0.0 all-gather.6.cloned.1.call-start
  6.5 2.0 copy.16
  8.6 0.0 copy-start.3
  8.6 0.0 all-gather.6.cloned.1.call-update
  8.6 0.0 all-gather.8.cloned.1.call-start
  8.7 0.9 copy.17
  9.6 21.9 %all_gather.19 = bf16[4,512,128]{2,0,1:T(4,128)(2,1)S(1)} all-gather(bf16[4,64,128]{2,0,1:T(4,128)(2,1)S(1)} %copy.17), channel_id=1, replica_groups=mesh['fs'=8,'tp'=4] {'fs'}, dimensions={1}, use_global_device_ids=true | all-gather | bytes 589824 | tf_op jit(solution)/shard_map/all_gather | solution.py:78
  31.4 1.1 copy.18
  32.6 0.0 all-gather.8.cloned.1.call-update
  32.6 0.0 all-gather.10.cloned.1.call-start
  32.6 0.7 all-gather.10.cloned.1.call-update
  33.3 0.0 all-gather.12.cloned.1.call-start
  33.4 0.5 all-gather.12.cloned.1.call-update
  33.9 0.0 all-gather.14.cloned.1.call-start
  33.9 0.5 all-gather.14.cloned.1.call-update
  34.5 0.0 reduce-scatter.2.cloned.1.call-start
  34.5 1.0 dynamic-slice_reduce_fusion.2
  35.6 0.3 broadcast_minimum_fusion
  35.9 0.0 all-gather.6.cloned.1.call-done
  36.0 2.1 fusion.3
  38.1 0.0 copy-done.3
  38.1 2.1 fusion.5
  40.2 3.1 reshape.110
  43.3 5.6 %fusion.9 = f32[4,128,2048]{1,0,2:T(4,128)S(1)} fusion(f32[4,128,2048]{1,0,2:T(4,128)} %reshape.110), kind=kLoop, calls=%fused_computation.20 | loop fusion | flops 1048576 | bytes 8388608 | tf_op jit(solution)/shard_map/add | solution.py:26
  48.9 2.3 fusion.10
  51.3 0.0 copy-start
  51.3 2.3 fusion.11
  53.6 0.1 copy-done
  53.8 16.8 %fusion.12 = bf16[4,128,2048]{1,0,2:T(4,128)(2,1)} fusion(f32[4,128,2048]{1,0,2:T(4,128)S(1)} %copy-done, f32[4,128,2048]{1,0,2:T(4,128)S(1)} %fusion.9, f32[4,128,2048]{1,0,2:T(4,128)S(1)} %fusion.11, f32[128,2048]{0,1:T(8,128)S(1)} %broadcast_minimum_fusion, pred[2048]{0:T(1024)(128)(4,1)S(1)} %get-tuple-element.11, ...), kind=kLoop, calls=%fused_computation.23 | loop fusion | flops 8388608 | bytes 15734784 | tf_op jit(solution)/shard_map/convert_element_type | solution.py:74
  70.6 2.7 reshape.102
  73.3 0.0 all-gather.8.cloned.1.call-done
  73.4 3.0 convolution_bitcast_fusion
  76.3 4.8 %copy.20 = f32[512,512,4]{0,2,1:T(4,128)} copy(f32[512,512,4]{0,1,2:T(8,128)S(1)} %convolution_bitcast_fusion) | data formatting | bytes 8388608 | tf_op jit(solution)/shard_map/tcg,gce->teg/transpose | solution.py:81
  81.1 0.0 copy-start.1
  81.1 0.0 copy-start.4
  81.1 5.5 %reshape.103 = f32[512,2048]{0,1:T(8,128)} reshape(f32[512,512,4]{0,2,1:T(4,128)} %copy.20) | data formatting | bytes 8388608 | tf_op jit(solution)/shard_map/reshape | solution.py:81
  86.5 0.0 copy-done.1
  86.6 0.0 copy-done.4
  86.6 0.0 copy-start.5
  86.6 2.8 fusion.6
  89.3 0.0 copy-start.2
  89.4 1.3 copy-done.2
  90.7 0.5 fusion
  91.2 67.5 %all-gather.10.cloned.1.call-done = bf16[2048,1408]{1,0:T(8,128)(2,1)} async-done(((bf16[256,1408]{1,0:T(8,128)(2,1)}), bf16[2048,1408]{1,0:T(8,128)(2,1)}) %all-gather.10.cloned.1.call-update) | async-done | bytes 5767184 | tf_op jit(solution)/shard_map/all_gather | solution.py:93
  158.8 0.0 copy-done.5
  158.8 6.9 %convolution_convert_fusion.1 = bf16[512,1408]{1,0:T(8,128)(2,1)S(1)} fusion(bf16[2048,1408]{1,0:T(8,128)(2,1)} %all-gather.10.cloned.1.call-done, bf16[512,2048]{0,1:T(8,128)(2,1)} %copy-done.2, f32[2048]{0:T(1024)S(1)} %copy-done.5, f32[512]{0:T(512)S(1)} %add_rsqrt_fusion), kind=kOutput, calls=%fused_computation.25 | convolution fusion | flops 2957705216 | bytes 9316352 | tf_op jit(solution)/shard_map/dot_general | solution.py:52
  165.7 0.2 convert.3
  165.9 85.4 %all-gather.12.cloned.1.call-done = bf16[2048,1408]{1,0:T(8,128)(2,1)} async-done(((bf16[256,1408]{1,0:T(8,128)(2,1)}), bf16[2048,1408]{1,0:T(8,128)(2,1)}) %all-gather.12.cloned.1.call-update) | async-done | bytes 5767184 | tf_op jit(solution)/shard_map/all_gather | solution.py:94
  251.3 6.9 %convolution_convert_fusion = bf16[512,1408]{1,0:T(8,128)(2,1)S(1)} fusion(bf16[2048,1408]{1,0:T(8,128)(2,1)} %all-gather.12.cloned.1.call-done, bf16[512,2048]{0,1:T(8,128)(2,1)} %copy-done.2, f32[2048]{0:T(1024)S(1)} %copy-done.5, f32[512]{0:T(512)S(1)} %add_rsqrt_fusion), kind=kOutput, calls=%fused_computation.24 | convolution fusion | flops 2957705216 | bytes 9316352 | tf_op jit(solution)/shard_map/dot_general | solution.py:52
  258.2 0.2 convert.4
  258.4 3.3 fusion.21
  261.8 82.8 %all-gather.14.cloned.1.call-done = bf16[1408,2048]{1,0:T(8,128)(2,1)} async-done(((bf16[1408,256]{1,0:T(8,128)(2,1)}), bf16[1408,2048]{1,0:T(8,128)(2,1)}) %all-gather.14.cloned.1.call-update) | async-done | bytes 5767184 | tf_op jit(solution)/shard_map/all_gather | solution.py:111
  344.6 8.5 %fusion.32 = f32[512,2048]{1,0:T(8,128)} fusion(bf16[512,1408]{1,0:T(8,128)(2,1)} %bitcast.18, bf16[1408,2048]{1,0:T(8,128)(2,1)} %all-gather.14.cloned.1.call-done), kind=kOutput, calls=%fused_computation.61 | convolution fusion | flops 2952790016 | bytes 11403264 | tf_op jit(solution)/shard_map/dot_general | solution.py:109
  353.1 0.0 reduce-scatter.2.cloned.1.call-update
  353.1 43.3 %reduce-scatter.2.cloned.1.call-done = f32[512,512]{1,0:T(8,128)} async-done(((f32[512,2048]{1,0:T(8,128)}), f32[512,512]{1,0:T(8,128)}) %reduce-scatter.2.cloned.1.call-update) | async-done | bytes 1048592 | tf_op jit(solution)/shard_map/reduce_scatter | solution.py:114
  396.4 2.1 convert_element_type.62
  (6 shorter events, 0.0 us)
Async XLA Ops:
  6.5 29.4 %all-gather.6.cloned.1.call-start = ((), (), s32[]{:S(2)}) async-start(), calls=%async_computation.1 | async-start | bytes 2621440 | tf_op jit(solution)/shard_map/all_gather | solution.py:69
  8.6 29.5 %copy-start.3 = (f32[2048]{0:T(1024)S(1)}, f32[2048]{0:T(1024)}, u32[]{:S(2)}) copy-start(f32[2048]{0:T(1024)} %param.11) | copy-start | bytes 24580
  8.6 64.7 %all-gather.8.cloned.1.call-start = ((), (), s32[]{:S(2)}) async-start(), calls=%async_computation.2 | async-start | bytes 2621440 | tf_op jit(solution)/shard_map/all_gather | solution.py:79
  32.6 126.2 %all-gather.10.cloned.1.call-start = ((), (), s32[]{:S(2)}) async-start(), calls=%async_computation.3 | async-start | bytes 6488064 | tf_op jit(solution)/shard_map/all_gather | solution.py:93
  33.3 218.0 %all-gather.12.cloned.1.call-start = ((), (), s32[]{:S(2)}) async-start(), calls=%async_computation.4 | async-start | bytes 6488064 | tf_op jit(solution)/shard_map/all_gather | solution.py:94
  33.9 310.7 %all-gather.14.cloned.1.call-start = ((), (), s32[]{:S(2)}) async-start(), calls=%async_computation.5 | async-start | bytes 6488064 | tf_op jit(solution)/shard_map/all_gather | solution.py:111
  34.5 361.9 %reduce-scatter.2.cloned.1.call-start = ((), (), s32[]{:S(2)}) async-start(), calls=%async_computation.6 | async-start | bytes 5242880 | tf_op jit(solution)/shard_map/reduce_scatter | solution.py:114
  51.3 2.5 copy-start
  81.1 5.5 %copy-start.1 = (bf16[512,2048]{0,1:T(8,128)(2,1)S(1)}, bf16[512,2048]{0,1:T(8,128)(2,1)}, u32[]{:S(2)}) copy-start(bf16[512,2048]{0,1:T(8,128)(2,1)} %all-gather.6.cloned.1.call-done) | copy-start | bytes 6291460
  81.1 5.5 %copy-start.4 = (f32[2048]{0:T(1024)S(1)}, f32[2048]{0:T(1024)}, u32[]{:S(2)}) copy-start(f32[2048]{0:T(1024)} %param.13) | copy-start | bytes 24580
  86.6 72.2 %copy-start.5 = (f32[2048]{0:T(1024)S(1)}, f32[2048]{0:T(1024)}, u32[]{:S(2)}) copy-start(f32[2048]{0:T(1024)} %param.14) | copy-start | bytes 24580
  89.3 1.3 copy-start.2
Sparse Core Ops, SparseCore 0:
  8.9 23.0 all-gather.5
  33.5 31.7 all-gather.7
  67.5 91.1 all-gather.9
  160.8 90.4 all-gather.11
  253.2 91.3 all-gather.13
  353.2 43.1 reduce-scatter.1
where the time goes:
time: 409 us; the launch traced here: 405 us
  waiting for transfers between devices  281 us (69%)
  other arithmetic  40.8 us (10%)
  matrix products  25.3 us (6%)
  local copies, waits for them, and re-layouts  22.7 us (6%)
  blocking collectives  21.9 us (5%)
  between operations  13.6 us (3%)
    all_gather x1, waiting for transfers between devices, body(): value_sum = add_single(lax.all_gather(up_weight, 'fs', axis=0, tiled=True))  85.4 us
    all_gather x1, waiting for transfers between devices, body(): lax.all_gather(down_weight, 'fs', axis=1, tiled=True)  82.8 us
    all_gather x1, waiting for transfers between devices, body(): gate_sum = add_single(lax.all_gather(gate_weight, 'fs', axis=0, tiled=True))  67.5 us
    reduce_scatter x1, waiting for transfers between devices, body(): lax.psum_scatter(partial_value, 'tp', scatter_dimension=1, tiled=True)  43.3 us
    all_gather x1, blocking collectives, body(): pool_part = lax.all_gather(pool_weight, 'fs', axis=1, tiled=True)  21.9 us
    convert_element_type x1, other arithmetic, body(): pool_less(normed.astype(jnp.float32).reshape(seq_count, LEN, channels))  16.8 us
    dot_general x2, matrix products, add_rows(): return jnp.dot(left, portion, preferred_element_type=jnp.float32)  13.8 us
    add x3, other arithmetic, pool_less(): running = running + delayed(running, amount)  10.3 us
  transfers between devices with their start and end apart: 6, of which 4 were waited for; matrix products, arithmetic and copies ran while one was open for 18% of the time, Pallas kernels for 0%

commit v1 on v0

v1 whole, which is shorter than its diff:
```python
import functools

import jax
import jax.numpy as jnp
from jax import lax
from jax.experimental import pallas as pl
from jax.experimental.pallas import tpu as pltpu
from jax.sharding import PartitionSpec as P

LEN = 128
GROUPS = 4
MESH = pl.DeviceIdType.MESH
epsilon = 1e-06

EARLY = (0, 1, 2, 3)
LATE = 4
CROSS = 5
FORE, BACK, SIDE = 0, 1, 2


def one_hot(rows, cols, hit):
    r = lax.broadcasted_iota(jnp.int32, (rows, cols), 0)
    c = lax.broadcasted_iota(jnp.int32, (rows, cols), 1)
    return jnp.where(hit(r, c), 1.0, 0.0).astype(jnp.bfloat16)


def delayed(values, amount):
    row = lax.broadcasted_iota(jnp.int32, values.shape, 0)
    return jnp.where(row < amount, 0.0, pltpu.roll(values, amount, 0))


def kernel(
    fs,
    tp,
    stream_ref,
    gain_mix_ref,
    pool_ref,
    pool_gain_ref,
    gain_ffn_ref,
    gate_ref,
    up_ref,
    gate_taps_ref,
    up_taps_ref,
    down_ref,
    out_ref,
    gate_all,
    up_all,
    down_all,
    pool_all,
    stream_all,
    middle_all,
    pooled,
    dense,
    normed_ffn,
    gate_sum,
    value_sum,
    hidden,
    part,
    theirs,
    total,
    w_send,
    w_recv,
    p_send,
    p_recv,
    a_send,
    a_recv,
    r_send,
    r_recv,
    own_sem,
):
    f = lax.axis_index("fs")
    t = lax.axis_index("tp")
    na = fs // 2
    a, b = f // 2, f % 2
    tokens, block = stream_ref.shape
    depth = gate_ref.shape[0]
    seqs = tokens // LEN
    cols = down_ref.shape[1]
    mate = t + 1 - 2 * (t % 2)

    barrier = pltpu.get_barrier_semaphore()
    for i in range(1, fs):
        pl.semaphore_signal(
            barrier, inc=1, device_id=(lax.rem(f + i, fs), t), device_id_type=MESH
        )
    for i in range(1, tp):
        pl.semaphore_signal(
            barrier, inc=1, device_id=(f, lax.rem(t + i, tp)), device_id_type=MESH
        )
    pl.semaphore_wait(barrier, fs + tp - 2)

    def act_copy(step, src, buf, owner, target):
        which = lax.rem(target - t + tp, tp)
        return pltpu.make_async_remote_copy(
            src_ref=src,
            dst_ref=buf.at[owner],
            send_sem=a_send.at[step, which, jnp.where(owner == t, 0, 1)],
            recv_sem=a_recv.at[step, owner],
            device_id=(f, target),
            device_id_type=MESH,
        )

    def act_start(step, src, buf):
        for i in range(2, tp, 2):
            act_copy(step, src, buf, t, lax.rem(t + i, tp)).start()
        act_copy(step, src, buf, t, mate).start()

    def act_relay(step, src, buf):
        for i in range(2, tp, 2):
            owner = lax.rem(t + i, tp)
            act_copy(step, buf.at[owner], buf, owner, mate).wait_recv()
            pltpu.make_async_remote_copy(
                src_ref=buf.at[owner],
                dst_ref=buf.at[owner],
                send_sem=a_send.at[step, i + 1, 1],
                recv_sem=a_recv.at[step, owner],
                device_id=(f, mate),
                device_id_type=MESH,
            ).start()
        for i in range(0, tp, 2):
            owner = lax.rem(mate + i, tp)
            act_copy(step, src, buf, owner, mate).wait_recv()

    def act_finish(step, src, buf):
        for i in range(2, tp, 2):
            act_copy(step, src, buf, t, lax.rem(t + i, tp)).wait_send()
            pltpu.make_async_remote_copy(
                src_ref=src,
                dst_ref=src,
                send_sem=a_send.at[step, i + 1, 1],
                recv_sem=a_recv.at[step, 0],
                device_id=(f, mate),
                device_id_type=MESH,
            ).wait_send()
        act_copy(step, src, buf, t, mate).wait_send()

    def pool_copy(target):
        return pltpu.make_async_remote_copy(
            src_ref=pool_ref,
            dst_ref=pool_all.at[f],
            send_sem=p_send.at[target],
            recv_sem=p_recv.at[f],
            device_id=(target, t),
            device_id_type=MESH,
        )

    act_start(0, stream_ref, stream_all)
    for i in range(1, fs):
        pool_copy(lax.rem(f + i, fs)).start()

    def slot(src, k):
        full = (gate_all, up_all, down_all)[k // 2]
        rows = full.shape[1] // 2
        return full.at[src, pl.ds((k % 2) * rows, rows)]

    def own(k):
        full = (gate_ref, up_ref, down_ref)[k // 2]
        rows = full.shape[0] // 2
        return full.at[pl.ds((k % 2) * rows, rows)]

    def piece(src, k, way, ref=None):
        target = (f + 2, f - 2, f + 1 - 2 * b)[way]
        return pltpu.make_async_remote_copy(
            src_ref=slot(src, k) if ref is None else ref,
            dst_ref=slot(src, k),
            send_sem=w_send.at[way, src, k],
            recv_sem=w_recv.at[src, k],
            device_id=(target, t),
            device_id_type=MESH,
        )

    def along(src, k, ref=None):
        @pl.when(a < na - 1)
        def _():
            piece(src, k, FORE, ref).start()

        @pl.when(a > 0)
        def _():
            piece(src, k, BACK, ref).start()

    pair = f + 1 - 2 * b
    piece(f, CROSS, SIDE, own(CROSS)).start()
    for k in EARLY:
        along(f, k, own(k))
        piece(f, k, SIDE, own(k)).start()
    locals_ = [
        pltpu.make_async_copy(stream_ref, stream_all.at[t], own_sem.at[0]),
        pltpu.make_async_copy(pool_ref, pool_all.at[f], own_sem.at[1]),
        pltpu.make_async_copy(gate_ref, gate_all.at[f], own_sem.at[2]),
        pltpu.make_async_copy(up_ref, up_all.at[f], own_sem.at[3]),
        pltpu.make_async_copy(down_ref, down_all.at[f], own_sem.at[4]),
    ]
    for copy in locals_:
        copy.start()

    def arrive(src, k, way):
        piece(src, k, way).wait_recv()
        if way == FORE:

            @pl.when(a < na - 1)
            def _():
                piece(src, k, FORE).start()

        else:

            @pl.when(a > 0)
            def _():
                piece(src, k, BACK).start()

    def events(d, ks):
        for k in ks:
            for way in (FORE, BACK):
                source = a - d if way == FORE else a + d

                @pl.when((source >= 0) & (source < na))
                def _():
                    src = source * 2 + b
                    arrive(src, k, way)
                    if k == CROSS:
                        arrive(source * 2 + 1 - b, k, way)
                    else:
                        piece(src, k, SIDE).start()

    for i in range(1, fs):
        src = lax.rem(f + i, fs)
        pltpu.make_async_remote_copy(
            src_ref=pool_ref,
            dst_ref=pool_all.at[src],
            send_sem=p_send.at[src],
            recv_sem=p_recv.at[src],
            device_id=(src, t),
            device_id_type=MESH,
        ).wait_recv()
    for copy in locals_:
        copy.wait()
    _, chans, outs = pool_ref.shape
    spread_rows = one_hot(
        GROUPS * chans,
        GROUPS * chans,
        lambda r, c: c == (r % GROUPS) * chans + r // GROUPS,
    )
    spread_cols = [
        one_hot(outs, GROUPS * outs, lambda r, c, g=g: c == r * GROUPS + g)
        for g in range(GROUPS)
    ]

    def densify(s, carry):
        wide = jnp.concatenate(
            [
                jnp.dot(
                    pool_all[s, g], spread_cols[g], preferred_element_type=jnp.float32
                )
                for g in range(GROUPS)
            ],
            axis=0,
        ).astype(jnp.bfloat16)
        rows = pl.ds(pl.multiple_of(s * GROUPS * chans, GROUPS * chans), GROUPS * chans)
        dense[rows, :] = jnp.dot(
            spread_rows, wide, preferred_element_type=jnp.float32
        ).astype(jnp.bfloat16)
        return carry

    lax.fori_loop(0, fs, densify, 0)

    act_relay(0, stream_ref, stream_all)

    def factor(buf, rows):
        square = jnp.zeros((LEN, 1), jnp.float32)
        for i in range(tp):
            v = buf[i, rows, :].astype(jnp.float32)
            square = square + jnp.sum(v * v, axis=-1, keepdims=True)
        return lax.rsqrt(square / (tp * block) + epsilon)

    def pool_seq(q, carry):
        rows = pl.ds(pl.multiple_of(q * LEN, LEN), LEN)
        scale = factor(stream_all, rows)
        lane = lax.broadcasted_iota(jnp.int32, (LEN, block), 1) % GROUPS
        row = lax.broadcasted_iota(jnp.int32, (LEN, block), 0)
        extent = jnp.where(lane == 0, 2, jnp.where(lane == 1, 4, jnp.where(lane == 2, 8, 16)))
        divisor = jnp.minimum(row + 1, extent).astype(jnp.float32)
        for i in range(tp):
            v = stream_all[i, rows, :].astype(jnp.float32)
            v = v * scale * gain_mix_ref[:, i * block : (i + 1) * block]
            v = v.astype(jnp.bfloat16).astype(jnp.float32)
            running = v + delayed(v, 1)
            picked = running
            for g, amount in ((1, 2), (2, 4), (3, 8)):
                running = running + delayed(running, amount)
                picked = jnp.where(lane >= g, running, picked)
            pooled[rows, i * block : (i + 1) * block] = (picked / divisor - v).astype(
                jnp.bfloat16
            )
        return carry

    lax.fori_loop(0, seqs, pool_seq, 0)

    def mix_seq(q, carry):
        rows = pl.ds(pl.multiple_of(q * LEN, LEN), LEN)
        mixed = jnp.dot(pooled[rows, :], dense[...], preferred_element_type=jnp.float32)
        total[rows, :] = (
            stream_ref[rows, :].astype(jnp.float32) + mixed * pool_gain_ref[...]
        ).astype(jnp.bfloat16)
        return carry

    lax.fori_loop(0, seqs, mix_seq, 0)

    act_start(1, total, middle_all)
    keep = pltpu.make_async_copy(total, middle_all.at[t], own_sem.at[0])
    keep.start()
    events(1, EARLY)
    gate_sum[...] = jnp.zeros_like(gate_sum)
    value_sum[...] = jnp.zeros_like(value_sum)
    keep.wait()
    act_relay(1, total, middle_all)

    def norm_seq(q, carry):
        rows = pl.ds(pl.multiple_of(q * LEN, LEN), LEN)
        scale = factor(middle_all, rows)
        for i in range(tp):
            span = slice(i * block, (i + 1) * block)
            v = middle_all[i, rows, :].astype(jnp.float32)
            normed_ffn[rows, span] = (v * scale * gain_ffn_ref[:, span]).astype(jnp.bfloat16)
        return carry

    lax.fori_loop(0, seqs, norm_seq, 0)

    def sources(d, take):
        def one(i, carry):
            far, up = i // 2, i % 2
            dist = d - far
            source = a + (2 * up - 1) * dist
            src = source * 2 + b + far - 2 * b * far
            exists = (source >= 0) & (source < na) & (dist >= 0) & (dist < na)

            @pl.when(exists & ((dist > 0) | (up == 0)))
            def _():
                take(src, source, far)

            return carry

        lax.fori_loop(0, 4, one, 0)

    half = tokens // 2

    def project(src, source, far):
        @pl.when(far == 1)
        def _():
            for k in EARLY:
                piece(src, k, SIDE).wait_recv()

        span = pl.ds(pl.multiple_of(src * depth, depth), depth)

        def chunk(m, carry):
            rows = pl.ds(pl.multiple_of(m * half, half), half)
            left = normed_ffn[rows, span]
            gate_sum[rows, :] += jnp.dot(
                left, gate_all[src], preferred_element_type=jnp.float32
            )
            value_sum[rows, :] += jnp.dot(
                left, up_all[src], preferred_element_type=jnp.float32
            )
            return carry

        lax.fori_loop(0, 2, chunk, 0)

    def late_start():
        along(f, LATE, own(LATE))
        piece(f, LATE, SIDE, own(LATE)).start()
        along(f, CROSS, own(CROSS))
        piece(pair, CROSS, SIDE).wait_recv()
        along(pair, CROSS)

    def early_round(d, carry):
        @pl.when((d >= 1) & (d <= na - 2))
        def _():
            events(d + 1, EARLY)

        @pl.when(d == na - 2)
        def _():
            late_start()

        @pl.when(d >= na - 1)
        def _():
            events(d - na + 2, (LATE, CROSS))

        sources(d, project)
        return carry

    lax.fori_loop(0, na + 1, early_round, 0)

    def gate_seq(q, carry):
        rows = pl.ds(pl.multiple_of(q * LEN, LEN), LEN)

        def conv(sums, taps):
            v = sums[rows, :].astype(jnp.bfloat16).astype(jnp.float32)
            reach = taps.shape[0]
            running = v * taps[reach - 1 : reach, :]
            for i in range(1, reach):
                running = running + delayed(v, i) * taps[reach - 1 - i : reach - i, :]
            return running

        gate = conv(gate_sum, gate_taps_ref)
        value = conv(value_sum, up_taps_ref)
        hidden[rows, :] = (gate / (1.0 + jnp.exp(-gate)) * value).astype(jnp.bfloat16)
        return carry

    lax.fori_loop(0, seqs, gate_seq, 0)

    def part_copy(src, source, col):
        return pltpu.make_async_remote_copy(
            src_ref=part.at[src],
            dst_ref=theirs.at[t, col],
            send_sem=r_send.at[src],
            recv_sem=r_recv.at[t, col],
            device_id=(f, source),
            device_id_type=MESH,
        )

    def finish(src, source, far):
        @pl.when(far == 1)
        def _():
            piece(src, LATE, SIDE).wait_recv()

        part[src] = jnp.dot(
            hidden[...], down_all[src], preferred_element_type=jnp.float32
        ).astype(jnp.bfloat16)

        @pl.when(source != t)
        def _():
            part_copy(src, source, src % 2).start()

    def late_round(d, carry):
        @pl.when((d >= 2) & (d + 1 < na))
        def _():
            events(d + 1, (LATE,))

        @pl.when((d >= 3) & (d < na))
        def _():
            events(d, (CROSS,))

        sources(d, finish)
        return carry

    lax.fori_loop(0, na + 1, late_round, 0)

    for col in range(2):
        for i in range(1, tp):
            peer = lax.rem(t + i, tp)
            pltpu.make_async_remote_copy(
                src_ref=part.at[0],
                dst_ref=theirs.at[peer, col],
                send_sem=r_send.at[0],
                recv_sem=r_recv.at[peer, col],
                device_id=(f, peer),
                device_id_type=MESH,
            ).wait_recv()
        summed = part[2 * t + col].astype(jnp.float32)
        for i in range(1, tp):
            summed = summed + theirs[lax.rem(t + i, tp), col].astype(jnp.float32)
        out_ref[:, col * cols : (col + 1) * cols] = summed.astype(out_ref.dtype)

    for i in range(1, fs):
        pool_copy(lax.rem(f + i, fs)).wait_send()
    act_finish(0, stream_ref, stream_all)
    act_finish(1, total, middle_all)

    def drain(s, carry):
        for k in range(6):
            line, col = s // 2, s % 2
            mine = (col == b) | (k == CROSS)

            @pl.when(mine & (a < na - 1) & (line <= a))
            def _():
                piece(s, k, FORE).wait_send()

            @pl.when(mine & (a > 0) & (line >= a))
            def _():
                piece(s, k, BACK).wait_send()

            @pl.when((s == f) if k == CROSS else (col == b))
            def _():
                piece(s, k, SIDE).wait_send()

        @pl.when(s // 2 != t)
        def _():
            part_copy(s, s // 2, s % 2).wait_send()

        return carry

    lax.fori_loop(0, fs, drain, 0)


def body(
    fs,
    tp,
    stream,
    gain_mix,
    pool_weight,
    pool_gain,
    gain_ffn,
    gate_weight,
    up_weight,
    gate_taps,
    up_taps,
    down_weight,
):
    tokens, block = stream.shape
    depth, width = gate_weight.shape
    cols = down_weight.shape[1]
    channels = gain_mix.shape[0]
    t = lax.axis_index("tp")

    def mine(values, size):
        return lax.dynamic_slice_in_dim(values, t * size, size, values.ndim - 1)

    bf16, f32 = jnp.bfloat16, jnp.float32
    dma = pltpu.SemaphoreType.DMA
    return pl.pallas_call(
        functools.partial(kernel, fs, tp),
        out_shape=jax.ShapeDtypeStruct((tokens, block), bf16),
        in_specs=[pl.BlockSpec(memory_space=pltpu.VMEM)] * 10,
        out_specs=pl.BlockSpec(memory_space=pltpu.VMEM),
        scratch_shapes=[
            pltpu.VMEM((fs, depth, width), bf16),
            pltpu.VMEM((fs, depth, width), bf16),
            pltpu.VMEM((fs, width, cols), bf16),
            pltpu.VMEM((fs,) + pool_weight.shape, bf16),
            pltpu.VMEM((tp, tokens, block), bf16),
            pltpu.VMEM((tp, tokens, block), bf16),
            pltpu.VMEM((tokens, channels), bf16),
            pltpu.VMEM((channels, block), bf16),
            pltpu.VMEM((tokens, channels), bf16),
            pltpu.VMEM((tokens, width), f32),
            pltpu.VMEM((tokens, width), f32),
            pltpu.VMEM((tokens, width), bf16),
            pltpu.VMEM((fs, tokens, cols), bf16),
            pltpu.VMEM((tp, 2, tokens, cols), bf16),
            pltpu.VMEM((tokens, block), bf16),
            dma((3, fs, 6)),
            dma((fs, 6)),
            dma((fs,)),
            dma((fs,)),
            dma((2, tp, 2)),
            dma((2, tp)),
            dma((fs,)),
            dma((tp, 2)),
            dma((5,)),
        ],
        compiler_params=pltpu.CompilerParams(
            collective_id=0, has_side_effects=True, vmem_limit_bytes=64 * 1024 * 1024 - 65536
        ),
    )(
        stream,
        gain_mix.reshape(1, channels),
        pool_weight,
        mine(pool_gain, block).reshape(1, block),
        gain_ffn.reshape(1, channels),
        gate_weight,
        up_weight,
        mine(gate_taps, width),
        mine(up_taps, width),
        down_weight,
    )


def solution(mesh):
    return jax.shard_map(
        functools.partial(body, mesh.shape["fs"], mesh.shape["tp"]),
        mesh=mesh,
        in_specs=(
            P("fs", "tp"),
            P(),
            P(None, "fs", "tp"),
            P(),
            P(),
            P("fs", "tp"),
            P("fs", "tp"),
            P(),
            P(),
            P("tp", "fs"),
        ),
        out_specs=P("fs", "tp"),
        check_vma=False,
    )
```

time: 409 us -> 205 us (0.50)
  the two profiles are of different devices: /device:TPU:21 before, /device:TPU:0 now
where the time goes in v1:
time: 205 us
  Pallas kernels  200 us (98%)
  local copies, waits for them, and re-layouts  4.56 us (2%)
    pallas_call x1, Pallas kernels, body(): pl.pallas_call(functools.partial(kernel, fs, tp), out_shape=jax.ShapeDtyp...  200 us

profile of v1, /device:TPU:0, one launch (start us, length us, event | category | flops | bytes accessed | tf_op | source)
XLA Modules:
  0.0 204.9 jit_solution(15420449391871745470)
XLA Ops:
  0.0 1.3 dynamic_slice.9
  1.3 1.4 constant_dynamic-slice_fusion
  2.7 200.3 %shard_map.100 = bf16[512,512]{1,0:T(8,128)(2,1)} custom-call(bf16[512,512]{1,0:T(8,128)(2,1)} %stream_ref.1, f32[1,2048]{1,0:T(1,128)} %bitcast.3, bf16[4,64,128]{2,1,0:T(8,128)(2,1)} %pool_ref.1, f32[1,512]{1,0:T(1,128)} %bitcast.5, f32[1,2048]{1,0:T(1,128)} %bitcast.4, bf16[256,1408]{1,0:T(8,128)(2,1)} %gate_ref.1, bf16[256,1408]{1,0:T(8,128)(2,1)} %up_ref.1, ...), custom_call_target="tpu_custom_call" | custom-call | tf_op jit(solution)/shard_map/pallas_call | solution.py:518
  203.0 1.9 copy.12

commit v2 on v1

--- a/solution.py
+++ b/solution.py
@@ -490,6 +490,523 @@
     lax.fori_loop(0, fs, drain, 0)
 
 
+MAIN, MATE, ACROSS = 0, 1, 2
+
+
+def split_kernel(
+    fs,
+    tp,
+    stream_ref,
+    gain_mix_ref,
+    pool_ref,
+    pool_gain_ref,
+    gain_ffn_ref,
+    gate_ref,
+    up_ref,
+    gate_taps_ref,
+    up_taps_ref,
+    down_ref,
+    out_ref,
+    gate_all,
+    up_all,
+    down_all,
+    pool_all,
+    stream_all,
+    middle_all,
+    pooled,
+    dense,
+    normed_ffn,
+    gate_sum,
+    value_sum,
+    hidden,
+    part,
+    mate_part,
+    y_own,
+    y_part,
+    z_own,
+    z_part,
+    total,
+    w_send,
+    w_recv,
+    p_send,
+    p_recv,
+    a_send,
+    a_recv,
+    b_sem,
+    m_send,
+    m_recv,
+    y_sem,
+    z_sem,
+    own_sem,
+):
+    f = lax.axis_index("fs")
+    t = lax.axis_index("tp")
+    a, b = f // 2, f % 2
+    tokens, block = stream_ref.shape
+    depth, width = gate_ref.shape
+    held = gate_all.shape[2]
+    other = width - held
+    seqs = tokens // LEN
+    cols = down_ref.shape[1]
+    mate = t + 1 - 2 * (t % 2)
+    across_y = lax.rem(t + 2, tp)
+    h = a // 2
+    has_mid = t % 2 == h
+    near = a + 1 - 2 * (a % 2)
+    far_in, far_out = 2 - h, 3 * (1 - h)
+    inner = (a == 1) | (a == 2)
+    partner = lax.rem(f + fs // 2, fs)
+    pair = f + 1 - 2 * b
+
+    barrier = pltpu.get_barrier_semaphore()
+    for i in range(1, fs):
+        pl.semaphore_signal(
+            barrier, inc=1, device_id=(lax.rem(f + i, fs), t), device_id_type=MESH
+        )
+    for i in range(1, tp):
+        pl.semaphore_signal(
+            barrier, inc=1, device_id=(f, lax.rem(t + i, tp)), device_id_type=MESH
+        )
+    pl.semaphore_wait(barrier, fs + tp - 2)
+
+    def act_view(step):
+        if step == 0:
+            return lambda owner: stream_all.at[owner]
+        return lambda owner: middle_all.at[owner, pl.ds((step - 1) * tokens, tokens)]
+
+    def act_copy(step, src, owner, target, role):
+        return pltpu.make_async_remote_copy(
+            src_ref=src,
+            dst_ref=act_view(step)(owner),
+            send_sem=a_send.at[step, role],
+            recv_sem=a_recv.at[step, owner],
+            device_id=(f, target),
+            device_id_type=MESH,
+        )
+
+    def act_start(step, src):
+        act_copy(step, src, t, across_y, 0).start()
+        act_copy(step, src, t, mate, 1).start()
+
+    def act_relay(step):
+        view = act_view(step)
+        act_copy(step, view(across_y), across_y, mate, 2).wait_recv()
+        act_copy(step, view(across_y), across_y, mate, 2).start()
+        act_copy(step, view(mate), mate, mate, 2).wait_recv()
+        diagonal = lax.rem(mate + 2, tp)
+        act_copy(step, view(diagonal), diagonal, mate, 2).wait_recv()
+
+    def act_finish(step):
+        view = act_view(step)
+        for role in range(3):
+            act_copy(step, view(t), t, mate, role).wait_send()
+
+    def pool_copy(target, owner):
+        return pltpu.make_async_remote_copy(
+            src_ref=pool_ref,
+            dst_ref=pool_all.at[owner],
+            send_sem=p_send.at[target],
+            recv_sem=p_recv.at[owner],
+            device_id=(target, t),
+            device_id_type=MESH,
+        )
+
+    act_start(0, stream_ref)
+    for i in range(1, fs):
+        pool_copy(lax.rem(f + i, fs), f).start()
+
+    def slot(src, k):
+        full = (gate_all, up_all, down_all)[k % 3]
+        span = pl.ds(0, other) if k < 3 else pl.ds(other, held - other)
+        if k % 3 == 2:
+            return full.at[src, span]
+        return full.at[src, :, span]
+
+    def own(q, k):
+        full = (gate_ref, up_ref, down_ref)[k % 3]
+        if k < 3:
+            span = pl.ds(pl.multiple_of(q * held, 128), other)
+        else:
+            span = pl.ds(other, held - other)
+        if k % 3 == 2:
+            return full.at[span]
+        return full.at[:, span]
+
+    def piece(src, k, way, ref=None):
+        target = (pair, near * 2 + b, far_in * 2 + b)[way]
+        return pltpu.make_async_remote_copy(
+            src_ref=slot(src, k) if ref is None else ref,
+            dst_ref=slot(src, k),
+            send_sem=w_send.at[way, src, k],
+            recv_sem=w_recv.at[src, k],
+            device_id=(target, t),
+            device_id_type=MESH,
+        )
+
+    def guarded(k, do):
+        if k < 3:
+            do()
+        else:
+            pl.when(has_mid)(do)
+
+    def own_start(k):
+        if k < 3:
+            piece(f, k, ACROSS, own(1 - h, k)).start()
+        else:
+
+            @pl.when(jnp.logical_not(has_mid))
+            def _():
+                piece(f, k, ACROSS, own(1 - h, k)).start()
+
+        def rest():
+            piece(f, k, MATE, own(h, k)).start()
+            piece(f, k, MAIN, own(h, k)).start()
+
+        guarded(k, rest)
+
+    def events(source, ks, passed):
+        src = source * 2 + b
+        for k in ks:
+
+            def one():
+                piece(src, k, MAIN).wait_recv()
+                if passed:
+
+                    @pl.when(inner)
+                    def _():
+                        piece(src, k, MATE).start()
+
+                piece(src, k, MAIN).start()
+
+            guarded(k, one)
+
+    def arrived(src, ks):
+        for k in ks:
+            guarded(k, lambda: piece(src, k, MAIN).wait_recv())
+
+    early, late = (0, 3, 1, 4), (2, 5)
+    for k in early:
+        own_start(k)
+
+    def local(k):
+        return pltpu.make_async_copy(own(h, k), slot(f, k), own_sem.at[k])
+
+    for k in range(6):
+        guarded(k, lambda: local(k).start())
+    keep_stream = pltpu.make_async_copy(stream_ref, stream_all.at[t], own_sem.at[6])
+    keep_pool = pltpu.make_async_copy(pool_ref, pool_all.at[f], own_sem.at[7])
+    keep_stream.start()
+    keep_pool.start()
+
+    @pl.when(jnp.logical_not(has_mid))
+    def _():
+        gate_all[:, :, other:] = jnp.zeros((fs, depth, held - other), jnp.bfloat16)
+        up_all[:, :, other:] = jnp.zeros((fs, depth, held - other), jnp.bfloat16)
+        down_all[:, other:, :] = jnp.zeros((fs, held - other, cols), jnp.bfloat16)
+
+    for i in range(1, fs):
+        src = lax.rem(f + i, fs)
+        pool_copy(src, src).wait_recv()
+    keep_pool.wait()
+    _, chans, outs = pool_ref.shape
+    spread_rows = one_hot(
+        GROUPS * chans,
+        GROUPS * chans,
+        lambda r, c: c == (r % GROUPS) * chans + r // GROUPS,
+    )
+    spread_cols = [
+        one_hot(outs, GROUPS * outs, lambda r, c, g=g: c == r * GROUPS + g)
+        for g in range(GROUPS)
+    ]
+
+    def densify(s, carry):
+        wide = jnp.concatenate(
+            [
+                jnp.dot(
+                    pool_all[s, g], spread_cols[g], preferred_element_type=jnp.float32
+                )
+                for g in range(GROUPS)
+            ],
+            axis=0,
+        ).astype(jnp.bfloat16)
+        rows = pl.ds(pl.multiple_of(s * GROUPS * chans, GROUPS * chans), GROUPS * chans)
+        dense[rows, :] = jnp.dot(
+            spread_rows, wide, preferred_element_type=jnp.float32
+        ).astype(jnp.bfloat16)
+        return carry
+
+    lax.fori_loop(0, fs, densify, 0)
+    keep_stream.wait()
+    act_relay(0)
+
+    def factor(buf, rows):
+        square = jnp.zeros((LEN, 1), jnp.float32)
+        for i in range(tp):
+            v = buf[i, rows, :].astype(jnp.float32)
+            square = square + jnp.sum(v * v, axis=-1, keepdims=True)
+        return lax.rsqrt(square / (tp * block) + epsilon)
+
+    def pool_seq(q, carry):
+        rows = pl.ds(pl.multiple_of(q * LEN, LEN), LEN)
+        scale = factor(stream_all, rows)
+        lane = lax.broadcasted_iota(jnp.int32, (LEN, block), 1) % GROUPS
+        row = lax.broadcasted_iota(jnp.int32, (LEN, block), 0)
+        extent = jnp.where(lane == 0, 2, jnp.where(lane == 1, 4, jnp.where(lane == 2, 8, 16)))
+        divisor = jnp.minimum(row + 1, extent).astype(jnp.float32)
+        for i in range(tp):
+            v = stream_all[i, rows, :].astype(jnp.float32)
+            v = v * scale * gain_mix_ref[:, i * block : (i + 1) * block]
+            v = v.astype(jnp.bfloat16).astype(jnp.float32)
+            running = v + delayed(v, 1)
+            picked = running
+            for g, amount in ((1, 2), (2, 4), (3, 8)):
+                running = running + delayed(running, amount)
+                picked = jnp.where(lane >= g, running, picked)
+            pooled[rows, i * block : (i + 1) * block] = (picked / divisor - v).astype(
+                jnp.bfloat16
+            )
+        mixed = jnp.dot(pooled[rows, :], dense[...], preferred_element_type=jnp.float32)
+        total[rows, :] = (
+            stream_ref[rows, :].astype(jnp.float32) + mixed * pool_gain_ref[...]
+        ).astype(jnp.bfloat16)
+        return carry
+
+    lax.fori_loop(0, seqs, pool_seq, 0)
+
+    to_partner = pltpu.make_async_remote_copy(
+        src_ref=total,
+        dst_ref=middle_all.at[t, pl.ds(tokens, tokens)],
+        send_sem=b_sem.at[0],
+        recv_sem=b_sem.at[1],
+        device_id=(partner, t),
+        device_id_type=MESH,
+    )
+    to_partner.start()
+    act_start(1, total)
+    keep = pltpu.make_async_copy(total, middle_all.at[t, pl.ds(0, tokens)], own_sem.at[8])
+    keep.start()
+    events(near, early, False)
+    keep.wait()
+    act_relay(1)
+
+    def norm(first):
+        def norm_seq(q, carry):
+            rows = pl.ds(pl.multiple_of(first + q * LEN, LEN), LEN)
+            scale = factor(middle_all, rows)
+            for i in range(tp):
+                span = slice(i * block, (i + 1) * block)
+                v = middle_all[i, rows, :].astype(jnp.float32)
+                normed_ffn[rows, span] = (v * scale * gain_ffn_ref[:, span]).astype(
+                    jnp.bfloat16
+                )
+            return carry
+
+        lax.fori_loop(0, seqs, norm_seq, 0)
+
+    norm(0)
+    events(far_in, early, True)
+    to_partner.wait_recv()
+    act_start(2, middle_all.at[t, pl.ds(tokens, tokens)])
+    events(far_out, early, True)
+    for k in late:
+        own_start(k)
+    for k in range(6):
+        guarded(k, lambda: local(k).wait())
+    act_relay(2)
+    norm(tokens)
+    arrived(pair, early)
+    for source in (near, far_in, far_out):
+        arrived(source * 2 + 1 - b, early)
+
+    chunk = 2 * LEN
+
+    def project(m, carry):
+        rows = pl.ds(pl.multiple_of(m * chunk, chunk), chunk)
+        left = normed_ffn[rows, :]
+        for full, sums in ((gate_all, gate_sum), (up_all, value_sum)):
+            sums[rows, :] = jnp.dot(
+                left,
+                full[...].reshape(fs * depth, held),
+                preferred_element_type=jnp.float32,
+            ).astype(jnp.bfloat16)
+        return carry
+
+    def gate_seq(q, carry):
+        rows = pl.ds(pl.multiple_of(q * LEN, LEN), LEN)
+
+        def conv(sums, taps_ref):
+            taps = jnp.concatenate(
+                [
+                    taps_ref[:, pl.ds(pl.multiple_of(h * held, 128), other)],
+                    taps_ref[:, other:held],
+                ],
+                axis=1,
+            )
+            v = sums[rows, :].astype(jnp.float32)
+            reach = taps.shape[0]
+            running = v * taps[reach - 1 : reach, :]
+            for i in range(1, reach):
+                running = running + delayed(v, i) * taps[reach - 1 - i : reach - i, :]
+            return running
+
+        gate = conv(gate_sum, gate_taps_ref)
+        value = conv(value_sum, up_taps_ref)
+        hidden[rows, :] = (gate / (1.0 + jnp.exp(-gate)) * value).astype(jnp.bfloat16)
+        return carry
+
+    chunks = tokens // chunk
+    lax.fori_loop(0, chunks, project, 0)
+    events(near, late, False)
+    lax.fori_loop(chunks, 2 * chunks, project, 0)
+    events(far_in, late, True)
+    lax.fori_loop(0, 2 * seqs, gate_seq, 0)
+
+    def source_of(i):
+        j, far = i // 2, i % 2
+        line = jnp.where(
+            j == 0, a, jnp.where(j == 1, near, jnp.where(j == 2, far_in, far_out))
+        )
+        return line, line * 2 + b + far - 2 * b * far, far
+
+    def mate_copy(s):
+        return pltpu.make_async_remote_copy(
+            src_ref=part.at[s],
+            dst_ref=mate_part.at[s],
+            send_sem=m_send.at[s],
+            recv_sem=m_recv.at[s],
+            device_id=(f, mate),
+            device_id_type=MESH,
+        )
+
+    def y_copy(col):
+        return pltpu.make_async_remote_copy(
+            src_ref=y_own.at[col],
+            dst_ref=y_part.at[col],
+            send_sem=y_sem.at[0, col],
+            recv_sem=y_sem.at[1, col],
+            device_id=(f, across_y),
+            device_id_type=MESH,
+        )
+
+    def z_copy(col):
+        return pltpu.make_async_remote_copy(
+            src_ref=z_own.at[col],
+            dst_ref=z_part.at[col],
+            send_sem=z_sem.at[0, col],
+            recv_sem=z_sem.at[1, col],
+            device_id=(partner, t),
+            device_id_type=MESH,
+        )
+
+    steps = 2 * fs // 2
+
+    def finish(i, carry):
+        @pl.when(i == 5)
+        def _():
+            events(far_out, late, True)
+
+        @pl.when(i < steps)
+        def _():
+            line, s, far = source_of(i)
+
+            @pl.when(far == 1)
+            def _():
+                arrived(s, late)
+
+            part[s] = jnp.dot(
+                hidden[...], down_all[s], preferred_element_type=jnp.float32
+            ).astype(jnp.bfloat16)
+
+            @pl.when(line % 2 != t % 2)
+            def _():
+                mate_copy(s).start()
+
+        @pl.when((i >= 1) & (i <= steps))
+        def _():
+            line, s, _ = source_of(i - 1)
+
+            @pl.when(line % 2 == t % 2)
+            def _():
+                mate_copy(s).wait_recv()
+
+                @pl.when(line != t)
+                def _():
+                    y_own[s % 2] = (
+                        part[s].astype(jnp.float32) + mate_part[s].astype(jnp.float32)
+                    ).astype(jnp.bfloat16)
+                    y_copy(s % 2).start()
+
+        @pl.when(i >= 2)
+        def _():
+            line, s, _ = source_of(i - 2)
+
+            @pl.when(line == t)
+            def _():
+                col = s % 2
+                y_copy(col).wait_recv()
+                theirs = pl.ds(tokens, tokens)
+                z_own[col] = (
+                    part[s, theirs, :].astype(jnp.float32)
+                    + mate_part[s, theirs, :].astype(jnp.float32)
+                    + y_part[col, theirs, :].astype(jnp.float32)
+                ).astype(jnp.bfloat16)
+                z_copy(col).start()
+
+        return carry
+
+    lax.fori_loop(0, steps + 2, finish, 0)
+
+    for col in range(2):
+        z_copy(col).wait_recv()
+        mine = pl.ds(0, tokens)
+        s = 2 * t + col
+        out_ref[:, col * cols : (col + 1) * cols] = (
+            part[s, mine, :].astype(jnp.float32)
+            + mate_part[s, mine, :].astype(jnp.float32)
+            + y_part[col, mine, :].astype(jnp.float32)
+            + z_part[col].astype(jnp.float32)
+        ).astype(out_ref.dtype)
+
+    for i in range(1, fs):
+        pool_copy(lax.rem(f + i, fs), f).wait_send()
+    for step in range(3):
+        act_finish(step)
+    to_partner.wait_send()
+    for col in range(2):
+        y_copy(col).wait_send()
+        z_copy(col).wait_send()
+
+    for k in range(6):
+        if k < 3:
+            piece(f, k, ACROSS, own(1 - h, k)).wait_send()
+        else:
+
+            @pl.when(jnp.logical_not(has_mid))
+            def _():
+                piece(f, k, ACROSS, own(1 - h, k)).wait_send()
+
+        def rest():
+            piece(f, k, MATE).wait_send()
+            for line in (a, near, far_in, far_out):
+                piece(line * 2 + b, k, MAIN).wait_send()
+
+            @pl.when(inner)
+            def _():
+                for line in (far_in, far_out):
+                    piece(line * 2 + b, k, MATE).wait_send()
+
+        guarded(k, rest)
+
+    def drain(s, carry):
+        @pl.when((s // 2) % 2 != t % 2)
+        def _():
+            mate_copy(s).wait_send()
+
+        return carry
+
+    lax.fori_loop(0, fs, drain, 0)
+
+
 def body(
     fs,
     tp,
@@ -515,12 +1032,46 @@
 
     bf16, f32 = jnp.bfloat16, jnp.float32
     dma = pltpu.SemaphoreType.DMA
-    return pl.pallas_call(
-        functools.partial(kernel, fs, tp),
-        out_shape=jax.ShapeDtypeStruct((tokens, block), bf16),
-        in_specs=[pl.BlockSpec(memory_space=pltpu.VMEM)] * 10,
-        out_specs=pl.BlockSpec(memory_space=pltpu.VMEM),
-        scratch_shapes=[
+    split = fs == 8 and tp == 4 and width % 256 == 128 and depth % 16 == 0
+    if split:
+        held = (width + 128) // 2
+        run = split_kernel
+        scratch = [
+            pltpu.VMEM((fs, depth, held), bf16),
+            pltpu.VMEM((fs, depth, held), bf16),
+            pltpu.VMEM((fs, held, cols), bf16),
+            pltpu.VMEM((fs,) + pool_weight.shape, bf16),
+            pltpu.VMEM((tp, tokens, block), bf16),
+            pltpu.VMEM((tp, 2 * tokens, block), bf16),
+            pltpu.VMEM((tokens, channels), bf16),
+            pltpu.VMEM((channels, block), bf16),
+            pltpu.VMEM((2 * tokens, channels), bf16),
+            pltpu.VMEM((2 * tokens, held), bf16),
+            pltpu.VMEM((2 * tokens, held), bf16),
+            pltpu.VMEM((2 * tokens, held), bf16),
+            pltpu.VMEM((fs, 2 * tokens, cols), bf16),
+            pltpu.VMEM((fs, 2 * tokens, cols), bf16),
+            pltpu.VMEM((2, 2 * tokens, cols), bf16),
+            pltpu.VMEM((2, 2 * tokens, cols), bf16),
+            pltpu.VMEM((2, tokens, cols), bf16),
+            pltpu.VMEM((2, tokens, cols), bf16),
+            pltpu.VMEM((tokens, block), bf16),
+            dma((3, fs, 6)),
+            dma((fs, 6)),
+            dma((fs,)),
+            dma((fs,)),
+            dma((3, 3)),
+            dma((3, tp)),
+            dma((2,)),
+            dma((fs,)),
+            dma((fs,)),
+            dma((2, 2)),
+            dma((2, 2)),
+            dma((9,)),
+        ]
+    else:
+        run = kernel
+        scratch = [
             pltpu.VMEM((fs, depth, width), bf16),
             pltpu.VMEM((fs, depth, width), bf16),
             pltpu.VMEM((fs, width, cols), bf16),
@@ -545,7 +1096,13 @@
             dma((fs,)),
             dma((tp, 2)),
             dma((5,)),
-        ],
+        ]
+    return pl.pallas_call(
+        functools.partial(run, fs, tp),
+        out_shape=jax.ShapeDtypeStruct((tokens, block), bf16),
+        in_specs=[pl.BlockSpec(memory_space=pltpu.VMEM)] * 10,
+        out_specs=pl.BlockSpec(memory_space=pltpu.VMEM),
+        scratch_shapes=scratch,
         compiler_params=pltpu.CompilerParams(
             collective_id=0, has_side_effects=True, vmem_limit_bytes=64 * 1024 * 1024 - 65536
         ),

time: 205 us -> 193 us (0.941)
  Pallas kernels: 200 us -> 189 us
    pallas_call x1, Pallas kernels: 200 us -> 189 us  [body(): pl.pallas_call(functools.partial(run, fs, tp), out_shape=jax.ShapeDtypeSt...]
where the time goes in v2:
time: 193 us
  Pallas kernels  189 us (98%)
  local copies, waits for them, and re-layouts  4.56 us (2%)
    pallas_call x1, Pallas kernels, body(): pl.pallas_call(functools.partial(run, fs, tp), out_shape=jax.ShapeDtypeSt...  189 us

profile of v2, /device:TPU:0, one launch (start us, length us, event | category | flops | bytes accessed | tf_op | source)
XLA Modules:
  0.0 193.2 jit_solution(10067088358862559387)
XLA Ops:
  0.0 1.3 dynamic_slice.9
  1.3 1.4 constant_dynamic-slice_fusion
  2.7 188.6 %shard_map.100 = bf16[512,512]{1,0:T(8,128)(2,1)} custom-call(bf16[512,512]{1,0:T(8,128)(2,1)} %stream_ref.1, f32[1,2048]{1,0:T(1,128)} %bitcast.3, bf16[4,64,128]{2,1,0:T(8,128)(2,1)} %pool_ref.1, f32[1,512]{1,0:T(1,128)} %bitcast.5, f32[1,2048]{1,0:T(1,128)} %bitcast.4, bf16[256,1408]{1,0:T(8,128)(2,1)} %gate_ref.1, bf16[256,1408]{1,0:T(8,128)(2,1)} %up_ref.1, ...), custom_call_target="tpu_custom_call" | custom-call | tf_op jit(solution)/shard_map/pallas_call | solution.py:1100
  191.3 1.9 copy.12

commit v3 on v2

--- a/solution.py
+++ b/solution.py
@@ -570,9 +570,8 @@
     pl.semaphore_wait(barrier, fs + tp - 2)
 
     def act_view(step):
-        if step == 0:
-            return lambda owner: stream_all.at[owner]
-        return lambda owner: middle_all.at[owner, pl.ds((step - 1) * tokens, tokens)]
+        buf = stream_all if step < 2 else middle_all
+        return lambda owner: buf.at[owner, pl.ds((step % 2) * tokens, tokens)]
 
     def act_copy(step, src, owner, target, role):
         return pltpu.make_async_remote_copy(
@@ -611,9 +610,30 @@
             device_id_type=MESH,
         )
 
+    to_partner = pltpu.make_async_remote_copy(
+        src_ref=stream_ref,
+        dst_ref=stream_all.at[t, pl.ds(tokens, tokens)],
+        send_sem=b_sem.at[0],
+        recv_sem=b_sem.at[1],
+        device_id=(partner, t),
+        device_id_type=MESH,
+    )
+
+    def pool_pass(owner, ref):
+        return pltpu.make_async_remote_copy(
+            src_ref=ref,
+            dst_ref=pool_all.at[owner],
+            send_sem=p_send.at[owner // 2 * 2 + 1 - b],
+            recv_sem=p_recv.at[owner],
+            device_id=(pair, t),
+            device_id_type=MESH,
+        )
+
     act_start(0, stream_ref)
-    for i in range(1, fs):
+    for i in range(2, fs, 2):
         pool_copy(lax.rem(f + i, fs), f).start()
+    pool_pass(f, pool_ref).start()
+    to_partner.start()
 
     def slot(src, k):
         full = (gate_all, up_all, down_all)[k % 3]
@@ -649,7 +669,7 @@
         else:
             pl.when(has_mid)(do)
 
-    def own_start(k):
+    def own_across(k):
         if k < 3:
             piece(f, k, ACROSS, own(1 - h, k)).start()
         else:
@@ -658,6 +678,7 @@
             def _():
                 piece(f, k, ACROSS, own(1 - h, k)).start()
 
+    def own_near(k):
         def rest():
             piece(f, k, MATE, own(h, k)).start()
             piece(f, k, MAIN, own(h, k)).start()
@@ -686,14 +707,19 @@
 
     early, late = (0, 3, 1, 4), (2, 5)
     for k in early:
-        own_start(k)
+        own_across(k)
+        own_near(k)
+    for k in late:
+        own_across(k)
 
     def local(k):
         return pltpu.make_async_copy(own(h, k), slot(f, k), own_sem.at[k])
 
     for k in range(6):
         guarded(k, lambda: local(k).start())
-    keep_stream = pltpu.make_async_copy(stream_ref, stream_all.at[t], own_sem.at[6])
+    keep_stream = pltpu.make_async_copy(
+        stream_ref, stream_all.at[t, pl.ds(0, tokens)], own_sem.at[6]
+    )
     keep_pool = pltpu.make_async_copy(pool_ref, pool_all.at[f], own_sem.at[7])
     keep_stream.start()
     keep_pool.start()
@@ -704,8 +730,12 @@
         up_all[:, :, other:] = jnp.zeros((fs, depth, held - other), jnp.bfloat16)
         down_all[:, other:, :] = jnp.zeros((fs, held - other, cols), jnp.bfloat16)
 
-    for i in range(1, fs):
+    for i in range(2, fs, 2):
         src = lax.rem(f + i, fs)
+        pool_copy(src, src).wait_recv()
+        pool_pass(src, pool_all.at[src]).start()
+    for i in range(0, fs, 2):
+        src = lax.rem(pair + i, fs)
         pool_copy(src, src).wait_recv()
     keep_pool.wait()
     _, chans, outs = pool_ref.shape
@@ -767,27 +797,28 @@
             )
         mixed = jnp.dot(pooled[rows, :], dense[...], preferred_element_type=jnp.float32)
         total[rows, :] = (
-            stream_ref[rows, :].astype(jnp.float32) + mixed * pool_gain_ref[...]
+            stream_all[t, rows, :].astype(jnp.float32)
+            + mixed * pool_gain_ref[:, pl.ds(pl.multiple_of(t * block, 128), block)]
         ).astype(jnp.bfloat16)
         return carry
 
     lax.fori_loop(0, seqs, pool_seq, 0)
-
-    to_partner = pltpu.make_async_remote_copy(
-        src_ref=total,
-        dst_ref=middle_all.at[t, pl.ds(tokens, tokens)],
-        send_sem=b_sem.at[0],
-        recv_sem=b_sem.at[1],
-        device_id=(partner, t),
-        device_id_type=MESH,
-    )
-    to_partner.start()
-    act_start(1, total)
-    keep = pltpu.make_async_copy(total, middle_all.at[t, pl.ds(0, tokens)], own_sem.at[8])
-    keep.start()
+    ours, theirs = pl.ds(0, tokens), pl.ds(tokens, tokens)
+    act_start(2, total.at[ours])
+    keep = [
+        pltpu.make_async_copy(total.at[span], middle_all.at[t, span], own_sem.at[8 + i])
+        for i, span in enumerate((ours, theirs))
+    ]
+    keep[0].start()
+    to_partner.wait_recv()
+    act_start(1, stream_all.at[t, theirs])
     events(near, early, False)
-    keep.wait()
     act_relay(1)
+    lax.fori_loop(seqs, 2 * seqs, pool_seq, 0)
+    act_start(3, total.at[theirs])
+    keep[1].start()
+    keep[0].wait()
+    act_relay(2)
 
     def norm(first):
         def norm_seq(q, carry):
@@ -803,17 +834,16 @@
 
         lax.fori_loop(0, seqs, norm_seq, 0)
 
+    events(far_in, early, True)
+    for k in late:
+        own_near(k)
     norm(0)
-    events(far_in, early, True)
-    to_partner.wait_recv()
-    act_start(2, middle_all.at[t, pl.ds(tokens, tokens)])
+    keep[1].wait()
+    act_relay(3)
+    norm(tokens)
     events(far_out, early, True)
-    for k in late:
-        own_start(k)
     for k in range(6):
         guarded(k, lambda: local(k).wait())
-    act_relay(2)
-    norm(tokens)
     arrived(pair, early)
     for source in (near, far_in, far_out):
         arrived(source * 2 + 1 - b, early)
@@ -837,8 +867,8 @@
         def conv(sums, taps_ref):
             taps = jnp.concatenate(
                 [
-                    taps_ref[:, pl.ds(pl.multiple_of(h * held, 128), other)],
-                    taps_ref[:, other:held],
+                    taps_ref[:, pl.ds(pl.multiple_of(t * width + h * held, 128), other)],
+                    taps_ref[:, pl.ds(pl.multiple_of(t * width + other, 128), held - other)],
                 ],
                 axis=1,
             )
@@ -862,9 +892,11 @@
     lax.fori_loop(0, 2 * seqs, gate_seq, 0)
 
     def source_of(i):
-        j, far = i // 2, i % 2
+        far = jnp.where((i == 2) | (i == 4) | (i == 5) | (i == 7), 1, 0)
         line = jnp.where(
-            j == 0, a, jnp.where(j == 1, near, jnp.where(j == 2, far_in, far_out))
+            (i == 0) | (i == 2),
+            a,
+            jnp.where((i == 3) | (i == 4), near, jnp.where(i >= 6, far_out, far_in)),
         )
         return line, line * 2 + b + far - 2 * b * far, far
 
@@ -901,7 +933,7 @@
     steps = 2 * fs // 2
 
     def finish(i, carry):
-        @pl.when(i == 5)
+        @pl.when(i == 4)
         def _():
             events(far_out, late, True)
 
@@ -944,7 +976,6 @@
             def _():
                 col = s % 2
                 y_copy(col).wait_recv()
-                theirs = pl.ds(tokens, tokens)
                 z_own[col] = (
                     part[s, theirs, :].astype(jnp.float32)
                     + mate_part[s, theirs, :].astype(jnp.float32)
@@ -967,9 +998,11 @@
             + z_part[col].astype(jnp.float32)
         ).astype(out_ref.dtype)
 
-    for i in range(1, fs):
+    for i in range(2, fs, 2):
         pool_copy(lax.rem(f + i, fs), f).wait_send()
-    for step in range(3):
+    for i in range(0, fs, 2):
+        pool_pass(lax.rem(f + i, fs), pool_ref).wait_send()
+    for step in range(4):
         act_finish(step)
     to_partner.wait_send()
     for col in range(2):
@@ -1041,9 +1074,9 @@
             pltpu.VMEM((fs, depth, held), bf16),
             pltpu.VMEM((fs, held, cols), bf16),
             pltpu.VMEM((fs,) + pool_weight.shape, bf16),
-            pltpu.VMEM((tp, tokens, block), bf16),
             pltpu.VMEM((tp, 2 * tokens, block), bf16),
-            pltpu.VMEM((tokens, channels), bf16),
+            pltpu.VMEM((tp, 2 * tokens, block), bf16),
+            pltpu.VMEM((2 * tokens, channels), bf16),
             pltpu.VMEM((channels, block), bf16),
             pltpu.VMEM((2 * tokens, channels), bf16),
             pltpu.VMEM((2 * tokens, held), bf16),
@@ -1055,19 +1088,19 @@
             pltpu.VMEM((2, 2 * tokens, cols), bf16),
             pltpu.VMEM((2, tokens, cols), bf16),
             pltpu.VMEM((2, tokens, cols), bf16),
-            pltpu.VMEM((tokens, block), bf16),
+            pltpu.VMEM((2 * tokens, block), bf16),
             dma((3, fs, 6)),
             dma((fs, 6)),
             dma((fs,)),
             dma((fs,)),
-            dma((3, 3)),
-            dma((3, tp)),
+            dma((4, 3)),
+            dma((4, tp)),
             dma((2,)),
             dma((fs,)),
             dma((fs,)),
             dma((2, 2)),
             dma((2, 2)),
-            dma((9,)),
+            dma((10,)),
         ]
     else:
         run = kernel
@@ -1097,6 +1130,10 @@
             dma((tp, 2)),
             dma((5,)),
         ]
+
+    def whole(values, size):
+        return values if split else mine(values, size)
+
     return pl.pallas_call(
         functools.partial(run, fs, tp),
         out_shape=jax.ShapeDtypeStruct((tokens, block), bf16),
@@ -1110,12 +1147,12 @@
         stream,
         gain_mix.reshape(1, channels),
         pool_weight,
-        mine(pool_gain, block).reshape(1, block),
+        whole(pool_gain, block).reshape(1, -1),
         gain_ffn.reshape(1, channels),
         gate_weight,
         up_weight,
-        mine(gate_taps, width),
-        mine(up_taps, width),
+        whole(gate_taps, width),
+        whole(up_taps, width),
         down_weight,
     )
 

time: 193 us -> 190 us (0.984)
  the two profiles are of different devices: /device:TPU:0 before, /device:TPU:21 now
where the time goes in v3:
time: 190 us
  Pallas kernels  188 us (99%)
    pallas_call x1, Pallas kernels, body(): pl.pallas_call(functools.partial(run, fs, tp), out_shape=jax.ShapeDtypeSt...  188 us

profile of v3, /device:TPU:21, one launch (start us, length us, event | category | flops | bytes accessed | tf_op | source)
XLA Modules:
  0.0 190.1 jit_solution(1306714493227395811)
XLA Ops:
  0.0 188.2 %shard_map.100 = bf16[512,512]{1,0:T(8,128)(2,1)} custom-call(bf16[512,512]{1,0:T(8,128)(2,1)} %stream_ref.1, f32[1,2048]{1,0:T(1,128)} %bitcast.3, bf16[4,64,128]{2,1,0:T(8,128)(2,1)} %pool_ref.1, f32[1,2048]{1,0:T(1,128)} %bitcast.4, f32[1,2048]{1,0:T(1,128)} %bitcast.5, bf16[256,1408]{1,0:T(8,128)(2,1)} %gate_ref.1, bf16[256,1408]{1,0:T(8,128)(2,1)} %up_ref.1, ...), custom_call_target="tpu_custom_call" | custom-call | tf_op jit(solution)/shard_map/pallas_call | solution.py:1137
  188.2 1.9 copy.12

commit v4 on v3

--- a/solution.py
+++ b/solution.py
@@ -555,6 +555,9 @@
     near = a + 1 - 2 * (a % 2)
     far_in, far_out = 2 - h, 3 * (1 - h)
     inner = (a == 1) | (a == 2)
+    first = jnp.where(inner, far_in, near)
+    second = jnp.where(inner, far_out, far_in)
+    third = jnp.where(inner, near, far_out)
     partner = lax.rem(f + fs // 2, fs)
     pair = f + 1 - 2 * b
 
@@ -633,7 +636,6 @@
     for i in range(2, fs, 2):
         pool_copy(lax.rem(f + i, fs), f).start()
     pool_pass(f, pool_ref).start()
-    to_partner.start()
 
     def slot(src, k):
         full = (gate_all, up_all, down_all)[k % 3]
@@ -679,23 +681,21 @@
                 piece(f, k, ACROSS, own(1 - h, k)).start()
 
     def own_near(k):
-        def rest():
-            piece(f, k, MATE, own(h, k)).start()
-            piece(f, k, MAIN, own(h, k)).start()
-
-        guarded(k, rest)
-
-    def events(source, ks, passed):
+        guarded(k, lambda: piece(f, k, MATE, own(h, k)).start())
+
+    def own_pair(k):
+        guarded(k, lambda: piece(f, k, MAIN, own(h, k)).start())
+
+    def events(source, ks):
         src = source * 2 + b
         for k in ks:
 
             def one():
                 piece(src, k, MAIN).wait_recv()
-                if passed:
-
-                    @pl.when(inner)
-                    def _():
-                        piece(src, k, MATE).start()
+
+                @pl.when(inner & (source // 2 != h))
+                def _():
+                    piece(src, k, MATE).start()
 
                 piece(src, k, MAIN).start()
 
@@ -706,11 +706,7 @@
             guarded(k, lambda: piece(src, k, MAIN).wait_recv())
 
     early, late = (0, 3, 1, 4), (2, 5)
-    for k in early:
-        own_across(k)
-        own_near(k)
-    for k in late:
-        own_across(k)
+    own_pair(early[0])
 
     def local(k):
         return pltpu.make_async_copy(own(h, k), slot(f, k), own_sem.at[k])
@@ -734,6 +730,17 @@
         src = lax.rem(f + i, fs)
         pool_copy(src, src).wait_recv()
         pool_pass(src, pool_all.at[src]).start()
+    to_partner.start()
+    for k in early:
+        own_across(k)
+
+    @pl.when(inner)
+    def _():
+        for k in early:
+            own_near(k)
+
+    for k in early[1:]:
+        own_pair(k)
     for i in range(0, fs, 2):
         src = lax.rem(pair + i, fs)
         pool_copy(src, src).wait_recv()
@@ -810,9 +817,23 @@
         for i, span in enumerate((ours, theirs))
     ]
     keep[0].start()
+
+    @pl.when(jnp.logical_not(inner))
+    def _():
+        for k in early:
+            own_near(k)
+
     to_partner.wait_recv()
     act_start(1, stream_all.at[t, theirs])
-    events(near, early, False)
+    events(first, early)
+
+    @pl.when(inner)
+    def _():
+        events(second, early)
+
+    for k in late:
+        own_across(k)
+
     act_relay(1)
     lax.fori_loop(seqs, 2 * seqs, pool_seq, 0)
     act_start(3, total.at[theirs])
@@ -834,14 +855,19 @@
 
         lax.fori_loop(0, seqs, norm_seq, 0)
 
-    events(far_in, early, True)
+
+    @pl.when(jnp.logical_not(inner))
+    def _():
+        events(second, early)
+
     for k in late:
         own_near(k)
+        own_pair(k)
     norm(0)
     keep[1].wait()
     act_relay(3)
     norm(tokens)
-    events(far_out, early, True)
+    events(third, early)
     for k in range(6):
         guarded(k, lambda: local(k).wait())
     arrived(pair, early)
@@ -886,9 +912,9 @@
 
     chunks = tokens // chunk
     lax.fori_loop(0, chunks, project, 0)
-    events(near, late, False)
+    events(first, late)
     lax.fori_loop(chunks, 2 * chunks, project, 0)
-    events(far_in, late, True)
+    events(second, late)
     lax.fori_loop(0, 2 * seqs, gate_seq, 0)
 
     def source_of(i):
@@ -896,7 +922,7 @@
         line = jnp.where(
             (i == 0) | (i == 2),
             a,
-            jnp.where((i == 3) | (i == 4), near, jnp.where(i >= 6, far_out, far_in)),
+            jnp.where((i == 3) | (i == 4), first, jnp.where(i >= 6, third, second)),
         )
         return line, line * 2 + b + far - 2 * b * far, far
 
@@ -935,7 +961,7 @@
     def finish(i, carry):
         @pl.when(i == 4)
         def _():
-            events(far_out, late, True)
+            events(third, late)
 
         @pl.when(i < steps)
         def _():

time: 190 us -> 191 us (level); the launches traced: 190 us -> 188 us
  Pallas kernels: 188 us -> 186 us
    pallas_call x1, Pallas kernels: 188 us -> 186 us  [body(): pl.pallas_call(functools.partial(run, fs, tp), out_shape=jax.ShapeDtypeSt...]
where the time goes in v4:
time: 191 us; the launch traced here: 188 us
  Pallas kernels  186 us (97%)
    pallas_call x1, Pallas kernels, body(): pl.pallas_call(functools.partial(run, fs, tp), out_shape=jax.ShapeDtypeSt...  186 us

profile of v4, /device:TPU:21, one launch (start us, length us, event | category | flops | bytes accessed | tf_op | source)
XLA Modules:
  0.0 187.7 jit_solution(17868078748496692085)
XLA Ops:
  0.0 185.8 %shard_map.100 = bf16[512,512]{1,0:T(8,128)(2,1)} custom-call(bf16[512,512]{1,0:T(8,128)(2,1)} %stream_ref.1, f32[1,2048]{1,0:T(1,128)} %bitcast.3, bf16[4,64,128]{2,1,0:T(8,128)(2,1)} %pool_ref.1, f32[1,2048]{1,0:T(1,128)} %bitcast.4, f32[1,2048]{1,0:T(1,128)} %bitcast.5, bf16[256,1408]{1,0:T(8,128)(2,1)} %gate_ref.1, bf16[256,1408]{1,0:T(8,128)(2,1)} %up_ref.1, ...), custom_call_target="tpu_custom_call" | custom-call | tf_op jit(solution)/shard_map/pallas_call | solution.py:1163
  185.8 1.9 copy.12

commit v5 on v4

--- a/solution.py
+++ b/solution.py
@@ -741,6 +741,8 @@
 
     for k in early[1:]:
         own_pair(k)
+    for k in late:
+        own_across(k)
     for i in range(0, fs, 2):
         src = lax.rem(pair + i, fs)
         pool_copy(src, src).wait_recv()
@@ -831,8 +833,6 @@
     def _():
         events(second, early)
 
-    for k in late:
-        own_across(k)
 
     act_relay(1)
     lax.fori_loop(seqs, 2 * seqs, pool_seq, 0)

time: 191 us -> 192 us (level)
  Pallas kernels: 186 us -> 188 us
where the time goes in v5:
time: 192 us; the launch traced here: 190 us
  Pallas kernels  188 us (98%)
    pallas_call x1, Pallas kernels, body(): pl.pallas_call(functools.partial(run, fs, tp), out_shape=jax.ShapeDtypeSt...  188 us

profile of v5, /device:TPU:21, one launch (start us, length us, event | category | flops | bytes accessed | tf_op | source)
XLA Modules:
  0.0 189.6 jit_solution(2793997410724496968)
XLA Ops:
  0.0 187.7 %shard_map.100 = bf16[512,512]{1,0:T(8,128)(2,1)} custom-call(bf16[512,512]{1,0:T(8,128)(2,1)} %stream_ref.1, f32[1,2048]{1,0:T(1,128)} %bitcast.3, bf16[4,64,128]{2,1,0:T(8,128)(2,1)} %pool_ref.1, f32[1,2048]{1,0:T(1,128)} %bitcast.4, f32[1,2048]{1,0:T(1,128)} %bitcast.5, bf16[256,1408]{1,0:T(8,128)(2,1)} %gate_ref.1, bf16[256,1408]{1,0:T(8,128)(2,1)} %up_ref.1, ...), custom_call_target="tpu_custom_call" | custom-call | tf_op jit(solution)/shard_map/pallas_call | solution.py:1163
  187.8 1.9 copy.12
